TPU v7x, 32 devices: a whole 2x2x4 slice. The times are simulated.
32 devices in a mesh: rep: 2 (over x), fs: 8 (over z, y), tp: 2 (over core).
Axes of the slice: x: 2, y: 2, z: 4, core: 2. Of those that a mesh axis runs over, the one named last changes fastest.
Arguments:
- tokens: bfloat16 [12288, 2048], P(('rep', 'fs'), 'tp'), may hold values from -6 to 6
- first_norm_gain: bfloat16 [2048], replicated, may hold values from 0.099609375 to 1.8984375
- query_projection_weight: bfloat16 [2048, 512], P('fs', 'tp'), may hold values from -0.125 to 0.125
- key_projection_weight: bfloat16 [2048, 512], P('fs', 'tp'), may hold values from -0.125 to 0.125
- value_projection_weight: bfloat16 [2048, 1024], P('fs', 'tp'), may hold values from -0.125 to 0.125
- output_gate_weight: bfloat16 [2048, 1024], P('fs', 'tp'), may hold values from -0.125 to 0.125
- decay_projection_weight: bfloat16 [2048, 512], P('fs', 'tp'), may hold values from -0.375 to 0.375
- fading_shift_vector: float32 [512], P('tp'), may hold values from -1 to 4
- added_fading_exponent: float32 [12288, 512], P(('rep', 'fs'), 'tp'), may hold values from -0.7 to 0
- per_head_gain: bfloat16 [128], replicated, may hold values from 0.099609375 to 1.8984375
- mixer_result_matrix: bfloat16 [1024, 2048], P('tp', 'fs'), may hold values from -0.1875 to 0.1875
- second_norm_gain: bfloat16 [2048], replicated, may hold values from 0.099609375 to 1.8984375
- up_linear_weight: bfloat16 [2048, 3072], P('fs', 'tp'), may hold values from -0.125 to 0.125
- up_gating_weight: bfloat16 [2048, 3072], P('fs', 'tp'), may hold values from -0.125 to 0.125
- depthwise_taps: bfloat16 [2, 3, 3072], P(None, None, 'tp'), may hold values from -3.5 to 3.5
- depthwise_bias: bfloat16 [2, 3072], P(None, 'tp'), may hold values from -3 to 3
- down_projection_weight: bfloat16 [3072, 2048], P('tp', 'fs'), may hold values from -0.109375 to 0.109375
Outputs:
- mixed: bfloat16 [12288, 2048], P(('rep', 'fs'), 'tp')
All inputs are finite; a program needn't handle non-finite values.
Results may differ from a plain program's by a relative error of at most 0.018.
Values may be sent and summed in bfloat16 or wider, within the bound.
A program may use at most 128 MiB of HBM per device.

v0:
```python
import jax
import jax.numpy as jnp
from jax import lax
from jax.sharding import PartitionSpec as P

KEY_DIM = 64
VALUE_DIM = 128
BLOCK = 64
SEQ_LEN = 256
norm_eps = 1e-06
fading_sharpness = 16.0


def normalize(source, gain):
    widened = source.astype(jnp.float32)
    scaled = widened * lax.rsqrt(jnp.mean(widened * widened, axis=-1, keepdims=True) + norm_eps)
    return (scaled * gain.astype(jnp.float32)).astype(jnp.bfloat16)


def direction(queries, key_heads, value_heads, fading_exponent):
    sequences, length, head_count, key_depth = queries.shape
    value_depth = value_heads.shape[-1]
    block_count = length // BLOCK
    query_blocks = queries.reshape(sequences, block_count, BLOCK, head_count, key_depth)
    key_blocks = key_heads.reshape(sequences, block_count, BLOCK, head_count, key_depth)
    value_blocks = value_heads.reshape(sequences, block_count, BLOCK, head_count, value_depth)
    cumulative = jnp.cumsum(
        fading_exponent.reshape(sequences, block_count, BLOCK, head_count, key_depth), axis=2
    )
    block_total = cumulative[:, :, -1:]
    query_decayed = query_blocks * jnp.exp(cumulative)
    key_inverse = key_blocks * jnp.exp(-cumulative)
    key_carried = key_blocks * jnp.exp(block_total - cumulative)
    lower_mask = jnp.tril(jnp.ones((BLOCK, BLOCK), dtype=bool))
    scores = jnp.einsum(
        "snihd,snjhd->snhij", query_decayed, key_inverse, precision=lax.Precision.HIGHEST
    )
    scores = jnp.where(lower_mask, scores, 0.0)
    within_block = jnp.einsum(
        "snhij,snjhv->snihv", scores, value_blocks, precision=lax.Precision.HIGHEST
    )
    increments = jnp.einsum(
        "snchd,snchv->nshdv", key_carried, value_blocks, precision=lax.Precision.HIGHEST
    )
    carry_decay = jnp.moveaxis(jnp.exp(block_total[:, :, 0]), 1, 0)

    def advance(running, inputs):
        factor, update = inputs
        return (factor[..., None] * running + update, running)

    initial = jnp.zeros((sequences, head_count, key_depth, value_depth), jnp.float32)
    unused, previous = lax.scan(advance, initial, (carry_decay, increments))
    across_blocks = jnp.einsum(
        "snchd,nshdv->snchv", query_decayed, previous, precision=lax.Precision.HIGHEST
    )
    return (within_block + across_blocks).reshape(sequences, length, head_count, value_depth)


def mixer_heads(queries_raw, keys_raw, values_raw, gates_raw, fading_exponent, per_head_gain):
    row_count = queries_raw.shape[0]
    head_count = values_raw.shape[1] // VALUE_DIM
    key_shape = (row_count // SEQ_LEN, SEQ_LEN, head_count, KEY_DIM)
    value_shape = (row_count // SEQ_LEN, SEQ_LEN, head_count, VALUE_DIM)
    queries = queries_raw.astype(jnp.float32).reshape(key_shape) * KEY_DIM ** (-0.5)
    key_heads = keys_raw.astype(jnp.float32).reshape(key_shape)
    value_heads = values_raw.astype(jnp.float32).reshape(value_shape)
    decay_heads = fading_exponent.reshape(key_shape)
    forward = direction(queries, key_heads, value_heads, decay_heads)
    backward = direction(
        jnp.flip(queries, 1),
        jnp.flip(key_heads, 1),
        jnp.flip(value_heads, 1),
        jnp.flip(decay_heads, 1),
    )
    attention = forward + jnp.flip(backward, 1)
    scaled = attention * lax.rsqrt(
        jnp.mean(attention * attention, axis=-1, keepdims=True) + norm_eps
    )
    scaled = scaled * per_head_gain.astype(jnp.float32)
    merged = scaled.reshape(row_count, head_count * VALUE_DIM)
    return (merged * jax.nn.silu(gates_raw.astype(jnp.float32))).astype(jnp.bfloat16)


def depthwise(linear_out, gated_out, depthwise_taps, depthwise_bias):
    row_count, channels = linear_out.shape

    def smooth(source, taps, offset_bias):
        framed = source.astype(jnp.float32).reshape(row_count // SEQ_LEN, SEQ_LEN, channels)
        tap_count = taps.shape[0]
        leading_zero_fill = tap_count // 2
        padded = jnp.pad(
            framed, ((0, 0), (leading_zero_fill, tap_count - 1 - leading_zero_fill), (0, 0))
        )
        result = offset_bias.astype(jnp.float32)
        for shift_index in range(tap_count):
            result = result + padded[:, shift_index : shift_index + SEQ_LEN] * taps[
                shift_index
            ].astype(jnp.float32)
        return result

    linear_conv = smooth(linear_out, depthwise_taps[0], depthwise_bias[0])
    gate_conv = smooth(gated_out, depthwise_taps[1], depthwise_bias[1])
    return (linear_conv * jax.nn.silu(gate_conv)).astype(jnp.bfloat16).reshape(row_count, channels)


def fold_rows(source, weight_pieces):
    return tuple(
        (
            jnp.dot(source, weight_piece, preferred_element_type=jnp.float32)
            for weight_piece in weight_pieces
        )
    )


def emit_with(source, weight_piece):
    return jnp.dot(source, weight_piece, preferred_element_type=jnp.float32)


def local(
    tokens,
    first_norm_gain,
    query_projection_weight,
    key_projection_weight,
    value_projection_weight,
    output_gate_weight,
    decay_projection_weight,
    fading_shift_vector,
    added_fading_exponent,
    per_head_gain,
    mixer_result_matrix,
    second_norm_gain,
    up_linear_weight,
    up_gating_weight,
    depthwise_taps,
    depthwise_bias,
    down_projection_weight,
):
    whole_rows = lax.all_gather(tokens, "tp", axis=1, tiled=True)
    normed = normalize(whole_rows, first_norm_gain)
    mapped_token_matrix = fold_rows(
        normed,
        (
            lax.all_gather(query_projection_weight, "fs", axis=0, tiled=True),
            lax.all_gather(key_projection_weight, "fs", axis=0, tiled=True),
            lax.all_gather(value_projection_weight, "fs", axis=0, tiled=True),
            lax.all_gather(output_gate_weight, "fs", axis=0, tiled=True),
            lax.all_gather(decay_projection_weight, "fs", axis=0, tiled=True),
        ),
    )
    queries_raw = mapped_token_matrix[0].astype(jnp.bfloat16)
    keys_raw = mapped_token_matrix[1].astype(jnp.bfloat16)
    values_raw = mapped_token_matrix[2].astype(jnp.bfloat16)
    gates_raw = mapped_token_matrix[3].astype(jnp.bfloat16)
    fading_exponent = (
        jax.nn.log_sigmoid(mapped_token_matrix[4] + fading_shift_vector) / fading_sharpness
        + added_fading_exponent
    )
    mixed_heads = mixer_heads(
        queries_raw, keys_raw, values_raw, gates_raw, fading_exponent, per_head_gain
    )
    mixer_terms = emit_with(
        mixed_heads, lax.all_gather(mixer_result_matrix, "fs", axis=1, tiled=True)
    )
    feature_share = tokens.shape[1]
    summed = lax.psum(mixer_terms.astype(jnp.bfloat16), "tp").astype(jnp.float32)
    full_after = (whole_rows.astype(jnp.float32) + summed).astype(jnp.bfloat16)
    after_mixer = lax.dynamic_slice_in_dim(
        full_after, lax.axis_index("tp") * feature_share, feature_share, 1
    )
    normed_two = normalize(full_after, second_norm_gain)
    upward = fold_rows(
        normed_two,
        (
            lax.all_gather(up_linear_weight, "fs", axis=0, tiled=True),
            lax.all_gather(up_gating_weight, "fs", axis=0, tiled=True),
        ),
    )
    linear_out = upward[0].astype(jnp.bfloat16)
    gated_out = upward[1].astype(jnp.bfloat16)
    hidden = depthwise(linear_out, gated_out, depthwise_taps, depthwise_bias)
    channel_terms = emit_with(
        hidden, lax.all_gather(down_projection_weight, "fs", axis=1, tiled=True)
    )
    channel_part = lax.psum_scatter(
        channel_terms.astype(jnp.bfloat16), "tp", scatter_dimension=1, tiled=True
    ).astype(jnp.float32)
    return (after_mixer.astype(jnp.float32) + channel_part).astype(jnp.bfloat16)


def solution(mesh):
    return jax.shard_map(
        local,
        mesh=mesh,
        in_specs=(
            P(("rep", "fs"), "tp"),
            P(),
            P("fs", "tp"),
            P("fs", "tp"),
            P("fs", "tp"),
            P("fs", "tp"),
            P("fs", "tp"),
            P("tp"),
            P(("rep", "fs"), "tp"),
            P(),
            P("tp", "fs"),
            P(),
            P("fs", "tp"),
            P("fs", "tp"),
            P(None, None, "tp"),
            P(None, "tp"),
            P("tp", "fs"),
        ),
        out_specs=P(("rep", "fs"), "tp"),
        check_vma=False,
    )
```

profile of v0, /device:TPU:0, one launch (start us, length us, event | category | flops | bytes accessed | tf_op | source)
XLA Modules:
  0.0 659.0 jit_solution(8518647654533081212)
XLA Ops:
  11.8 11.9 %all-gather.11.cloned.1.call-done = bf16[768,2048]{1,0:T(8,128)(2,1)} async-done(((bf16[768,1024]{1,0:T(8,128)(2,1)}), bf16[768,2048]{1,0:T(8,128)(2,1)}) %all-gather.11.cloned.1.call-update) | async-done | bytes 3145744 | tf_op jit(solution)/shard_map/all_gather | solution.py:138
  23.8 2.6 fusion.3
  26.3 41.0 %all-gather.17.cloned.1.call-done = bf16[2048,256]{1,0:T(8,128)(2,1)} async-done(((bf16[256,256]{1,0:T(8,128)(2,1)}), bf16[2048,256]{1,0:T(8,128)(2,1)}) %all-gather.17.cloned.1.call-update) | async-done | bytes 1048592 | tf_op jit(solution)/shard_map/all_gather | solution.py:147
  67.4 3.6 fusion.42
  73.4 35.2 %all-gather.19.cloned.1.call-done = bf16[2048,256]{1,0:T(8,128)(2,1)} async-done(((bf16[256,256]{1,0:T(8,128)(2,1)}), bf16[2048,256]{1,0:T(8,128)(2,1)}) %all-gather.19.cloned.1.call-update) | async-done | bytes 1048592 | tf_op jit(solution)/shard_map/all_gather | solution.py:144
  108.5 3.2 fusion.36
  111.7 1.8 reshape_reshape.11
  115.1 1.3 rev.19
  119.4 30.1 %all-gather.15.cloned.1.call-done = bf16[2048,256]{1,0:T(8,128)(2,1)} async-done(((bf16[256,256]{1,0:T(8,128)(2,1)}), bf16[2048,256]{1,0:T(8,128)(2,1)}) %all-gather.15.cloned.1.call-update) | async-done | bytes 1048592 | tf_op jit(solution)/shard_map/all_gather | solution.py:143
  149.5 3.2 broadcast_multiply_fusion.1
  152.7 1.8 mul.209
  156.4 1.6 copy.100
  158.3 1.3 rev.20
  159.7 1.8 copy.87
  161.5 4.8 exponential_multiply_fusion.3
  166.3 3.8 fusion.20
  170.1 2.6 exponential_multiply_fusion.1
  173.9 3.8 fusion.16
  177.7 21.6 %all-gather.13.cloned.1.call-done = bf16[2048,512]{1,0:T(8,128)(2,1)} async-done(((bf16[256,512]{1,0:T(8,128)(2,1)}), bf16[2048,512]{1,0:T(8,128)(2,1)}) %all-gather.13.cloned.1.call-update) | async-done | bytes 2097168 | tf_op jit(solution)/shard_map/all_gather | solution.py:145
  199.3 5.3 convolution_convert_fusion.5
  204.6 1.7 reshape_reshape.9
  206.4 2.8 reshape.131
  209.2 4.0 fusion.18
  214.6 8.1 %while.26 = (s32[]{:T(128)}, f32[3,4,64,128]{3,2,1,0:T(8,128)S(1)}, f32[4,3,4,64,128]{4,3,2,0,1:T(8,128)}, f32[4,3,4,64]{3,2,0,1:T(4,128)S(1)}, f32[4,3,4,64,128]{4,3,2,1,0:T(8,128)}, /*index=5*/s32[]{:T(128)}, s32[]{:T(128)}) while((s32[]{:T(128)}, f32[3,4,64,128]{3,2,1,0:T(8,128)S(1)}, f32[4,3,4,64,128]{4,3,2,0,1:T(8,128)}, ...), condition=%wide.region_3.4_spmd.clone, body=%wide.region_2.3_spmd.clone.sunk | while | flops 393219 | bytes 1975904 | solution.py:52
  222.8 2.5 fusion.23
  225.3 1.7 add_bitcast_fusion.1
  229.7 10.2 %rev.17 = f32[3,256,4,128]{3,1,2,0:T(8,128)S(1)} reverse(f32[3,256,4,128]{3,1,2,0:T(8,128)} %copy.79), dimensions={1} | reverse | bytes 3145728 | tf_op jit(solution)/shard_map/jit(_flip)/rev | solution.py:72
  239.9 5.3 fusion.11
  246.5 10.9 %while.27 = (s32[]{:T(128)}, f32[3,4,64,128]{3,2,1,0:T(8,128)S(1)}, f32[4,3,4,64,128]{4,3,2,0,1:T(8,128)}, f32[4,3,4,64]{3,2,0,1:T(4,128)}, f32[4,3,4,64,128]{4,3,2,1,0:T(8,128)}, /*index=5*/s32[]{:T(128)}, s32[]{:T(128)}) while((s32[]{:T(128)}, f32[3,4,64,128]{3,2,1,0:T(8,128)S(1)}, f32[4,3,4,64,128]{4,3,2,0,1:T(8,128)}, ...), condition=%wide.region_6.7_spmd.clone, body=%wide.region_5.6_spmd.clone.sunk | while | flops 393219 | bytes 1975904 | solution.py:52
  257.4 3.7 fusion.30
  261.1 1.7 add_bitcast_fusion
  264.1 10.6 %rev.21 = f32[3,256,4,128]{3,1,2,0:T(8,128)S(1)} reverse(f32[3,256,4,128]{3,1,2,0:T(8,128)} %bitcast.93), dimensions={1} | reverse | bytes 3145728 | tf_op jit(solution)/shard_map/jit(_flip)/rev | solution.py:75
  275.8 2.2 copy.97
  277.9 22.0 %all-gather.23.cloned.1.call-done = bf16[512,2048]{1,0:T(8,128)(2,1)} async-done(((bf16[512,256]{1,0:T(8,128)(2,1)}), bf16[512,2048]{1,0:T(8,128)(2,1)}) %all-gather.23.cloned.1.call-update) | async-done | bytes 2097168 | tf_op jit(solution)/shard_map/all_gather | solution.py:162
  299.9 8.1 %convolution_convert_fusion = bf16[768,2048]{1,0:T(8,128)(2,1)} fusion(bf16[512,2048]{1,0:T(8,128)(2,1)} %all-gather.23.cloned.1.call-done, f32[96,8,4,128]{3,2,1,0:T(4,128)} %bitcast.99, bf16[2048,512]{1,0:T(8,128)(2,1)} %all-gather.21.cloned.1.call-done, bf16[768,2048]{1,0:T(8,128)(2,1)S(1)} %copy-done.2, f32[2048]{0:T(1024)S(1)} %convert_element_type.115, ...), kind=kOutput, calls=%fused_computation.19 | convolution fusion | flops 3232235520 | bytes 12069888 | tf_op jit(solution)/shard_map/dot_general | solution.py:116
  310.3 19.3 %all-reduce.4.cloned.1.call-done = bf16[768,2048]{1,0:T(8,128)(2,1)} async-done(((bf16[768,2048]{1,0:T(8,128)(2,1)}), bf16[768,2048]{1,0:T(8,128)(2,1)}) %all-reduce.4.cloned.1.call-update) | async-done | bytes 3145744 | tf_op jit(solution)/shard_map/psum | solution.py:165
  329.6 5.1 fusion
  334.7 97.0 %all-gather.25.cloned.1.call-done = bf16[2048,1536]{1,0:T(8,128)(2,1)} async-done(((bf16[256,1536]{1,0:T(8,128)(2,1)}), bf16[2048,1536]{1,0:T(8,128)(2,1)}) %all-gather.25.cloned.1.call-update) | async-done | bytes 6291472 | tf_op jit(solution)/shard_map/all_gather | solution.py:174
  431.7 8.9 %convolution_convert_fusion.2 = bf16[768,1536]{1,0:T(8,128)(2,1)S(1)} fusion(bf16[2048,1536]{1,0:T(8,128)(2,1)} %all-gather.25.cloned.1.call-done, bf16[768,2048]{1,0:T(8,128)(2,1)} %get-tuple-element.166, f32[2048]{0:T(1024)S(1)} %convert_element_type.133, f32[768]{0:T(1024)S(1)} %add_rsqrt_fusion.1), kind=kOutput, calls=%fused_computation.21 | convolution fusion | flops 4839309312 | bytes 11807744 | tf_op jit(solution)/shard_map/dot_general | solution.py:109
  440.7 2.8 convert.11
  443.5 87.2 %all-gather.27.cloned.1.call-done = bf16[2048,1536]{1,0:T(8,128)(2,1)} async-done(((bf16[256,1536]{1,0:T(8,128)(2,1)}), bf16[2048,1536]{1,0:T(8,128)(2,1)}) %all-gather.27.cloned.1.call-update) | async-done | bytes 6291472 | tf_op jit(solution)/shard_map/all_gather | solution.py:175
  530.7 8.2 %convolution_convert_fusion.1 = bf16[768,1536]{1,0:T(8,128)(2,1)S(1)} fusion(bf16[2048,1536]{1,0:T(8,128)(2,1)} %all-gather.27.cloned.1.call-done, bf16[768,2048]{1,0:T(8,128)(2,1)S(1)} %copy-done.3, f32[2048]{0:T(1024)S(1)} %convert_element_type.133, f32[768]{0:T(1024)S(1)} %add_rsqrt_fusion.1), kind=kOutput, calls=%fused_computation.20 | convolution fusion | flops 4839309312 | bytes 11807744 | tf_op jit(solution)/shard_map/dot_general | solution.py:109
  539.5 1.9 copy-done
  541.4 5.3 multiply_convert_fusion
  546.7 83.7 %all-gather.29.cloned.1.call-done = bf16[1536,2048]{1,0:T(8,128)(2,1)} async-done(((bf16[1536,256]{1,0:T(8,128)(2,1)}), bf16[1536,2048]{1,0:T(8,128)(2,1)}) %all-gather.29.cloned.1.call-update) | async-done | bytes 6291472 | tf_op jit(solution)/shard_map/all_gather | solution.py:182
  630.4 9.0 %convolution_convert_fusion.3 = bf16[768,2048]{1,0:T(8,128)(2,1)} fusion(bf16[768,1536]{1,0:T(8,128)(2,1)} %bitcast.98, bf16[1536,2048]{1,0:T(8,128)(2,1)} %all-gather.29.cloned.1.call-done), kind=kOutput, calls=%fused_computation.22 | convolution fusion | flops 4833411072 | bytes 11796480 | tf_op jit(solution)/shard_map/dot_general | solution.py:116
  639.5 9.3 %reduce-scatter.2.cloned.1.call-done = bf16[768,1024]{1,0:T(8,128)(2,1)} async-done(((bf16[768,2048]{1,0:T(8,128)(2,1)}), bf16[768,1024]{1,0:T(8,128)(2,1)}) %reduce-scatter.2.cloned.1.call-update) | async-done | bytes 1572880 | tf_op jit(solution)/shard_map/reduce_scatter | solution.py:184
  648.8 3.2 add_convert_fusion
  (129 shorter events, 44.8 us)
Async XLA Ops:
  6.5 4.8 copy-start.15
  6.5 4.8 copy-start.22
  6.5 17.2 %all-gather.11.cloned.1.call-start = ((), (), s32[]{:S(2)}) async-start(), calls=%async_computation.1 | async-start | bytes 4718592 | tf_op jit(solution)/shard_map/all_gather | solution.py:138
  7.3 60.1 %all-gather.17.cloned.1.call-start = ((), (), s32[]{:S(2)}) async-start(), calls=%async_computation.4 | async-start | bytes 1179648 | tf_op jit(solution)/shard_map/all_gather | solution.py:147
  8.0 100.5 %all-gather.19.cloned.1.call-start = ((), (), s32[]{:S(2)}) async-start(), calls=%async_computation.5 | async-start | bytes 1179648 | tf_op jit(solution)/shard_map/all_gather | solution.py:144
  8.7 140.8 %all-gather.15.cloned.1.call-start = ((), (), s32[]{:S(2)}) async-start(), calls=%async_computation.3 | async-start | bytes 1179648 | tf_op jit(solution)/shard_map/all_gather | solution.py:143
  9.3 190.0 %all-gather.13.cloned.1.call-start = ((), (), s32[]{:S(2)}) async-start(), calls=%async_computation.2 | async-start | bytes 2359296 | tf_op jit(solution)/shard_map/all_gather | solution.py:145
  9.9 268.0 %all-gather.21.cloned.1.call-start = ((), (), s32[]{:S(2)}) async-start(), calls=%async_computation.6 | async-start | bytes 2359296 | tf_op jit(solution)/shard_map/all_gather | solution.py:146
  10.5 289.4 %all-gather.23.cloned.1.call-start = ((), (), s32[]{:S(2)}) async-start(), calls=%async_computation.7 | async-start | bytes 2359296 | tf_op jit(solution)/shard_map/all_gather | solution.py:162
  11.2 318.4 %all-reduce.4.cloned.1.call-start = ((), (), s32[]{:S(2)}) async-start(), calls=%async_computation.8 | async-start | bytes 6291456 | tf_op jit(solution)/shard_map/psum | solution.py:165
  11.8 55.5 %copy-start.20 = (f32[768,256]{1,0:T(8,128)S(1)}, f32[768,256]{1,0:T(8,128)}, u32[]{:S(2)}) copy-start(f32[768,256]{1,0:T(8,128)} %param.29) | copy-start | bytes 2359300
  11.8 55.5 %copy-start.21 = (f32[256]{0:T(256)S(1)}, f32[256]{0:T(256)}, u32[]{:S(2)}) copy-start(f32[256]{0:T(256)} %param.28) | copy-start | bytes 3076
  26.3 173.0 %copy-start.17 = (f32[768]{0:T(1024)}, f32[768]{0:T(1024)S(1)}, u32[]{:S(2)}) copy-start(f32[768]{0:T(1024)S(1)} %add_rsqrt_fusion.2) | copy-start | bytes 9220
  71.9 1.2 copy-start.4
  117.6 1.1 copy-start.5
  156.4 1.6 copy-start.12
  166.3 3.8 copy-start.6
  166.3 3.8 copy-start.10
  166.3 3.8 copy-start.11
  172.7 1.1 copy-start.1
  222.7 2.5 copy-start.8
  226.9 1.4 copy-start.7
  257.4 3.7 copy-start.9
  274.7 0.6 copy-start.19
  275.3 24.6 %copy-start.18 = (f32[768]{0:T(1024)S(1)}, f32[768]{0:T(1024)}, u32[]{:S(2)}) copy-start(f32[768]{0:T(1024)} %copy-done.17) | copy-start | bytes 9220
  275.8 24.1 %copy-start.2 = (bf16[768,2048]{1,0:T(8,128)(2,1)S(1)}, bf16[768,2048]{1,0:T(8,128)(2,1)}, u32[]{:S(2)}) copy-start(bf16[768,2048]{1,0:T(8,128)(2,1)} %all-gather.11.cloned.1.call-done) | copy-start | bytes 9437188
  308.0 2.1 copy-start.16
  308.0 2.2 copy-start.14
  308.0 2.2 copy-start.13
  308.0 123.7 %all-gather.25.cloned.1.call-start = ((), (), s32[]{:S(2)}) async-start(), calls=%async_computation.9 | async-start | bytes 7077888 | tf_op jit(solution)/shard_map/all_gather | solution.py:174
  308.8 221.9 %all-gather.27.cloned.1.call-start = ((), (), s32[]{:S(2)}) async-start(), calls=%async_computation.10 | async-start | bytes 7077888 | tf_op jit(solution)/shard_map/all_gather | solution.py:175
  309.3 321.1 %all-gather.29.cloned.1.call-start = ((), (), s32[]{:S(2)}) async-start(), calls=%async_computation.11 | async-start | bytes 7077888 | tf_op jit(solution)/shard_map/all_gather | solution.py:182
  310.1 338.7 %reduce-scatter.2.cloned.1.call-start = ((), (), s32[]{:S(2)}) async-start(), calls=%async_computation.12 | async-start | bytes 4718592 | tf_op jit(solution)/shard_map/reduce_scatter | solution.py:184
  440.6 90.0 %copy-start.3 = (bf16[768,2048]{1,0:T(8,128)(2,1)S(1)}, bf16[768,2048]{1,0:T(8,128)(2,1)}, u32[]{:S(2)}) copy-start(bf16[768,2048]{1,0:T(8,128)(2,1)} %get-tuple-element.166) | copy-start | bytes 9437188
  538.9 2.5 copy-start
Sparse Core Ops, SparseCore 0:
  8.9 14.8 all-gather.10
  25.9 41.4 all-gather.16
  69.5 38.9 all-gather.18
  110.5 38.9 all-gather.14
  151.5 47.7 all-gather.12
  201.3 47.6 all-gather.20
  251.0 48.8 all-gather.22
  308.1 21.4 all-reduce.3
  331.8 99.8 all-gather.24
  433.8 96.8 all-gather.26
  532.7 97.6 all-gather.28
  639.6 9.1 reduce-scatter.1
where the time goes:
time: 669 us; the launch traced here: 659 us
  waiting for transfers between devices  465 us (70%)
  matrix products  76 us (11%)
  local copies, waits for them, and re-layouts  58.3 us (9%)
  other arithmetic  45.3 us (7%)
  between operations  14.2 us (2%)
    all_gather x1, waiting for transfers between devices, local(): lax.all_gather(up_linear_weight, 'fs', axis=0, tiled=True)  97 us
    all_gather x1, waiting for transfers between devices, local(): lax.all_gather(up_gating_weight, 'fs', axis=0, tiled=True)  87.2 us
    all_gather x1, waiting for transfers between devices, local(): lax.all_gather(down_projection_weight, 'fs', axis=1, tiled=True)  83.7 us
    all_gather x1, waiting for transfers between devices, local(): lax.all_gather(decay_projection_weight, 'fs', axis=0, tiled=True)  41 us
    all_gather x1, waiting for transfers between devices, local(): lax.all_gather(key_projection_weight, 'fs', axis=0, tiled=True)  35.2 us
    dot_general x6, matrix products, fold_rows(): jnp.dot(source, weight_piece, preferred_element_type=jnp.float32)  32.4 us
    all_gather x1, waiting for transfers between devices, local(): lax.all_gather(query_projection_weight, 'fs', axis=0, tiled=True)  30.1 us
    all_gather x1, waiting for transfers between devices, local(): lax.all_gather(mixer_result_matrix, 'fs', axis=1, tiled=True)  22 us
  transfers between devices with their start and end apart: 12, of which 11 were waited for; matrix products, arithmetic and copies ran while one was open for 23% of the time, Pallas kernels for 0%

commit v1 on v0

--- a/solution.py
+++ b/solution.py
@@ -179,7 +179,7 @@
     gated_out = upward[1].astype(jnp.bfloat16)
     hidden = depthwise(linear_out, gated_out, depthwise_taps, depthwise_bias)
     channel_terms = emit_with(
-        hidden, lax.all_gather(down_projection_weight, "fs", axis=1, tiled=True)
+        hidden, jnp.concatenate(lax.all_gather(down_projection_weight, "fs"), axis=1)
     )
     channel_part = lax.psum_scatter(
         channel_terms.astype(jnp.bfloat16), "tp", scatter_dimension=1, tiled=True

time: 669 us -> 686 us (1.025)
  other arithmetic: 45.3 us -> 53.7 us
    reshape x0 -> x1, local copies, waits for them, and re-layouts: none -> 8.64 us  [local(): jnp.concatenate(lax.all_gather(down_projection_weight, 'fs'), axis=1)]
  transfers between devices with their start and end apart: 12 -> 12, of which waited for: 11 -> 11; matrix products, arithmetic and copies ran while one was open for 23% -> 22% of each run, Pallas kernels for 0% -> 0%
where the time goes in v1:
time: 686 us; the launch traced here: 676 us
  waiting for transfers between devices  469 us (68%)
  matrix products  73.4 us (11%)
  local copies, waits for them, and re-layouts  65 us (9%)
  other arithmetic  53.7 us (8%)
  between operations  14.2 us (2%)
    all_gather x1, waiting for transfers between devices, local(): lax.all_gather(up_linear_weight, 'fs', axis=0, tiled=True)  97 us
    all_gather x1, waiting for transfers between devices, local(): lax.all_gather(down_projection_weight, 'fs')  88.1 us
    all_gather x1, waiting for transfers between devices, local(): lax.all_gather(up_gating_weight, 'fs', axis=0, tiled=True)  87.2 us
    all_gather x1, waiting for transfers between devices, local(): lax.all_gather(decay_projection_weight, 'fs', axis=0, tiled=True)  41 us
    all_gather x1, waiting for transfers between devices, local(): lax.all_gather(key_projection_weight, 'fs', axis=0, tiled=True)  35.2 us
    dot_general x6, matrix products, fold_rows(): jnp.dot(source, weight_piece, preferred_element_type=jnp.float32)  32.4 us
    all_gather x1, waiting for transfers between devices, local(): lax.all_gather(query_projection_weight, 'fs', axis=0, tiled=True)  30.1 us
    all_gather x1, waiting for transfers between devices, local(): lax.all_gather(mixer_result_matrix, 'fs', axis=1, tiled=True)  22 us
  transfers between devices with their start and end apart: 12, of which 11 were waited for; matrix products, arithmetic and copies ran while one was open for 22% of the time, Pallas kernels for 0%

profile of v1, /device:TPU:0, one launch (start us, length us, event | category | flops | bytes accessed | tf_op | source)
XLA Modules:
  0.0 676.0 jit_solution(11383684760207287242)
XLA Ops:
  11.8 11.9 %all-gather.12.cloned.1.call-done = bf16[768,2048]{1,0:T(8,128)(2,1)} async-done(((bf16[768,1024]{1,0:T(8,128)(2,1)}), bf16[768,2048]{1,0:T(8,128)(2,1)}) %all-gather.12.cloned.1.call-update) | async-done | bytes 3145744 | tf_op jit(solution)/shard_map/all_gather | solution.py:138
  23.8 2.6 fusion.3
  26.3 41.0 %all-gather.18.cloned.1.call-done = bf16[2048,256]{1,0:T(8,128)(2,1)} async-done(((bf16[256,256]{1,0:T(8,128)(2,1)}), bf16[2048,256]{1,0:T(8,128)(2,1)}) %all-gather.18.cloned.1.call-update) | async-done | bytes 1048592 | tf_op jit(solution)/shard_map/all_gather | solution.py:147
  67.4 3.6 fusion.42
  73.4 35.2 %all-gather.20.cloned.1.call-done = bf16[2048,256]{1,0:T(8,128)(2,1)} async-done(((bf16[256,256]{1,0:T(8,128)(2,1)}), bf16[2048,256]{1,0:T(8,128)(2,1)}) %all-gather.20.cloned.1.call-update) | async-done | bytes 1048592 | tf_op jit(solution)/shard_map/all_gather | solution.py:144
  108.5 3.2 fusion.36
  111.7 1.8 reshape_reshape.11
  115.1 1.3 rev.19
  119.4 30.1 %all-gather.16.cloned.1.call-done = bf16[2048,256]{1,0:T(8,128)(2,1)} async-done(((bf16[256,256]{1,0:T(8,128)(2,1)}), bf16[2048,256]{1,0:T(8,128)(2,1)}) %all-gather.16.cloned.1.call-update) | async-done | bytes 1048592 | tf_op jit(solution)/shard_map/all_gather | solution.py:143
  149.5 3.2 broadcast_multiply_fusion.1
  152.7 1.8 mul.209
  156.4 1.6 copy.102
  159.7 1.8 copy.88
  161.5 4.8 exponential_multiply_fusion.3
  166.3 3.8 fusion.20
  170.1 2.6 exponential_multiply_fusion.1
  173.9 3.8 fusion.16
  177.7 21.6 %all-gather.14.cloned.1.call-done = bf16[2048,512]{1,0:T(8,128)(2,1)} async-done(((bf16[256,512]{1,0:T(8,128)(2,1)}), bf16[2048,512]{1,0:T(8,128)(2,1)}) %all-gather.14.cloned.1.call-update) | async-done | bytes 2097168 | tf_op jit(solution)/shard_map/all_gather | solution.py:145
  199.3 5.3 convolution_convert_fusion.5
  204.6 1.7 reshape_reshape.9
  206.4 2.8 reshape.139
  209.2 4.0 fusion.18
  214.6 8.1 %while.26 = (s32[]{:T(128)}, f32[3,4,64,128]{3,2,1,0:T(8,128)S(1)}, f32[4,3,4,64,128]{4,3,2,0,1:T(8,128)}, f32[4,3,4,64]{3,2,0,1:T(4,128)S(1)}, f32[4,3,4,64,128]{4,3,2,1,0:T(8,128)}, /*index=5*/s32[]{:T(128)}, s32[]{:T(128)}) while((s32[]{:T(128)}, f32[3,4,64,128]{3,2,1,0:T(8,128)S(1)}, f32[4,3,4,64,128]{4,3,2,0,1:T(8,128)}, ...), condition=%wide.region_3.4_spmd.clone, body=%wide.region_2.3_spmd.clone.sunk | while | flops 393219 | bytes 1975904 | solution.py:52
  222.8 2.5 fusion.23
  225.3 1.7 add_bitcast_fusion.1
  229.7 10.2 %rev.17 = f32[3,256,4,128]{3,1,2,0:T(8,128)S(1)} reverse(f32[3,256,4,128]{3,1,2,0:T(8,128)} %copy.80), dimensions={1} | reverse | bytes 3145728 | tf_op jit(solution)/shard_map/jit(_flip)/rev | solution.py:72
  239.9 5.3 fusion.11
  246.5 10.9 %while.27 = (s32[]{:T(128)}, f32[3,4,64,128]{3,2,1,0:T(8,128)S(1)}, f32[4,3,4,64,128]{4,3,2,0,1:T(8,128)}, f32[4,3,4,64]{3,2,0,1:T(4,128)}, f32[4,3,4,64,128]{4,3,2,1,0:T(8,128)}, /*index=5*/s32[]{:T(128)}, s32[]{:T(128)}) while((s32[]{:T(128)}, f32[3,4,64,128]{3,2,1,0:T(8,128)S(1)}, f32[4,3,4,64,128]{4,3,2,0,1:T(8,128)}, ...), condition=%wide.region_6.7_spmd.clone, body=%wide.region_5.6_spmd.clone.sunk | while | flops 393219 | bytes 1975904 | solution.py:52
  257.4 3.7 fusion.30
  261.1 1.7 add_bitcast_fusion
  264.1 10.6 %rev.21 = f32[3,256,4,128]{3,1,2,0:T(8,128)S(1)} reverse(f32[3,256,4,128]{3,1,2,0:T(8,128)} %bitcast.99), dimensions={1} | reverse | bytes 3145728 | tf_op jit(solution)/shard_map/jit(_flip)/rev | solution.py:75
  275.8 2.2 copy.98
  277.9 22.0 %all-gather.24.cloned.1.call-done = bf16[512,2048]{1,0:T(8,128)(2,1)} async-done(((bf16[512,256]{1,0:T(8,128)(2,1)}), bf16[512,2048]{1,0:T(8,128)(2,1)}) %all-gather.24.cloned.1.call-update) | async-done | bytes 2097168 | tf_op jit(solution)/shard_map/all_gather | solution.py:162
  299.9 8.1 %convolution_convert_fusion = bf16[768,2048]{1,0:T(8,128)(2,1)} fusion(bf16[512,2048]{1,0:T(8,128)(2,1)} %all-gather.24.cloned.1.call-done, f32[96,8,4,128]{3,2,1,0:T(4,128)} %bitcast.105, bf16[2048,512]{1,0:T(8,128)(2,1)} %all-gather.22.cloned.1.call-done, bf16[768,2048]{1,0:T(8,128)(2,1)S(1)} %copy-done.1, f32[2048]{0:T(1024)S(1)} %convert_element_type.115, ...), kind=kOutput, calls=%fused_computation.19 | convolution fusion | flops 3232235520 | bytes 12069888 | tf_op jit(solution)/shard_map/dot_general | solution.py:116
  310.3 19.3 %all-reduce.4.cloned.1.call-done = bf16[768,2048]{1,0:T(8,128)(2,1)} async-done(((bf16[768,2048]{1,0:T(8,128)(2,1)}), bf16[768,2048]{1,0:T(8,128)(2,1)}) %all-reduce.4.cloned.1.call-update) | async-done | bytes 3145744 | tf_op jit(solution)/shard_map/psum | solution.py:165
  329.6 5.1 fusion
  334.7 97.0 %all-gather.26.cloned.1.call-done = bf16[2048,1536]{1,0:T(8,128)(2,1)} async-done(((bf16[256,1536]{1,0:T(8,128)(2,1)}), bf16[2048,1536]{1,0:T(8,128)(2,1)}) %all-gather.26.cloned.1.call-update) | async-done | bytes 6291472 | tf_op jit(solution)/shard_map/all_gather | solution.py:174
  431.7 8.9 %convolution_convert_fusion.2 = bf16[768,1536]{1,0:T(8,128)(2,1)S(1)} fusion(bf16[2048,1536]{1,0:T(8,128)(2,1)} %all-gather.26.cloned.1.call-done, bf16[768,2048]{1,0:T(8,128)(2,1)} %get-tuple-element.166, f32[2048]{0:T(1024)S(1)} %convert_element_type.133, f32[768]{0:T(1024)S(1)} %add_rsqrt_fusion.1), kind=kOutput, calls=%fused_computation.21 | convolution fusion | flops 4839309312 | bytes 11807744 | tf_op jit(solution)/shard_map/dot_general | solution.py:109
  440.7 2.8 convert.11
  443.5 87.2 %all-gather.28.cloned.1.call-done = bf16[2048,1536]{1,0:T(8,128)(2,1)} async-done(((bf16[256,1536]{1,0:T(8,128)(2,1)}), bf16[2048,1536]{1,0:T(8,128)(2,1)}) %all-gather.28.cloned.1.call-update) | async-done | bytes 6291472 | tf_op jit(solution)/shard_map/all_gather | solution.py:175
  530.7 8.2 %convolution_convert_fusion.1 = bf16[768,1536]{1,0:T(8,128)(2,1)S(1)} fusion(bf16[2048,1536]{1,0:T(8,128)(2,1)} %all-gather.28.cloned.1.call-done, bf16[768,2048]{1,0:T(8,128)(2,1)S(1)} %copy-done.2, f32[2048]{0:T(1024)S(1)} %convert_element_type.133, f32[768]{0:T(1024)S(1)} %add_rsqrt_fusion.1), kind=kOutput, calls=%fused_computation.20 | convolution fusion | flops 4839309312 | bytes 11807744 | tf_op jit(solution)/shard_map/dot_general | solution.py:109
  538.9 2.8 convert.12
  541.7 88.1 %all-gather.30.cloned.1.call-done = bf16[12288,256]{1,0:T(8,128)(2,1)} async-done(((bf16[1536,256]{1,0:T(8,128)(2,1)}), bf16[12288,256]{1,0:T(8,128)(2,1)}) %all-gather.30.cloned.1.call-update) | async-done | bytes 6291472 | tf_op jit(solution)/shard_map/all_gather | solution.py:182
  629.8 8.6 %copy.99 = bf16[1536,8,256]{0,2,1:T(8,128)(2,1)} copy(bf16[1536,8,256]{2,0,1:T(8,128)(2,1)} %bitcast.96) | data formatting | bytes 12582912 | tf_op jit(solution)/shard_map/reshape | solution.py:182
  638.4 11.5 %multiply_convert_fusion = bf16[3,256,1536]{2,1,0:T(8,128)(2,1)S(1)} fusion(f32[3,256,1536]{2,1,0:T(8,128)} %convert.12, f32[3,256,1536]{2,1,0:T(8,128)} %convert.11, f32[1536]{0:T(1024)S(1)} %get-tuple-element.141, f32[1536]{0:T(1024)S(1)} %get-tuple-element.142, f32[1536]{0:T(1024)S(1)} %get-tuple-element.138, f32[1536]{0:T(1024)S(1)} %get-tuple-element.144, ...), kind=kLoop, calls=%fused_computation.18 | loop fusion | flops 21233664 | bytes 11845632 | tf_op jit(solution)/shard_map/convert_element_type | solution.py:103
  650.0 6.5 convolution_convert_fusion.3
  656.5 9.3 %reduce-scatter.2.cloned.1.call-done = bf16[768,1024]{1,0:T(8,128)(2,1)} async-done(((bf16[768,2048]{1,0:T(8,128)(2,1)}), bf16[768,1024]{1,0:T(8,128)(2,1)}) %reduce-scatter.2.cloned.1.call-update) | async-done | bytes 1572880 | tf_op jit(solution)/shard_map/reduce_scatter | solution.py:184
  665.8 3.2 add_convert_fusion
  (130 shorter events, 45.5 us)
Async XLA Ops:
  6.5 4.8 copy-start.15
  6.5 4.8 copy-start.22
  6.5 17.2 %all-gather.12.cloned.1.call-start = ((), (), s32[]{:S(2)}) async-start(), calls=%async_computation.1 | async-start | bytes 4718592 | tf_op jit(solution)/shard_map/all_gather | solution.py:138
  7.3 60.1 %all-gather.18.cloned.1.call-start = ((), (), s32[]{:S(2)}) async-start(), calls=%async_computation.4 | async-start | bytes 1179648 | tf_op jit(solution)/shard_map/all_gather | solution.py:147
  8.0 100.5 %all-gather.20.cloned.1.call-start = ((), (), s32[]{:S(2)}) async-start(), calls=%async_computation.5 | async-start | bytes 1179648 | tf_op jit(solution)/shard_map/all_gather | solution.py:144
  8.7 140.8 %all-gather.16.cloned.1.call-start = ((), (), s32[]{:S(2)}) async-start(), calls=%async_computation.3 | async-start | bytes 1179648 | tf_op jit(solution)/shard_map/all_gather | solution.py:143
  9.3 190.0 %all-gather.14.cloned.1.call-start = ((), (), s32[]{:S(2)}) async-start(), calls=%async_computation.2 | async-start | bytes 2359296 | tf_op jit(solution)/shard_map/all_gather | solution.py:145
  9.9 268.0 %all-gather.22.cloned.1.call-start = ((), (), s32[]{:S(2)}) async-start(), calls=%async_computation.6 | async-start | bytes 2359296 | tf_op jit(solution)/shard_map/all_gather | solution.py:146
  10.5 289.4 %all-gather.24.cloned.1.call-start = ((), (), s32[]{:S(2)}) async-start(), calls=%async_computation.7 | async-start | bytes 2359296 | tf_op jit(solution)/shard_map/all_gather | solution.py:162
  11.2 318.4 %all-reduce.4.cloned.1.call-start = ((), (), s32[]{:S(2)}) async-start(), calls=%async_computation.8 | async-start | bytes 6291456 | tf_op jit(solution)/shard_map/psum | solution.py:165
  11.8 55.5 %copy-start.20 = (f32[768,256]{1,0:T(8,128)S(1)}, f32[768,256]{1,0:T(8,128)}, u32[]{:S(2)}) copy-start(f32[768,256]{1,0:T(8,128)} %param.29) | copy-start | bytes 2359300
  11.8 55.5 %copy-start.21 = (f32[256]{0:T(256)S(1)}, f32[256]{0:T(256)}, u32[]{:S(2)}) copy-start(f32[256]{0:T(256)} %param.28) | copy-start | bytes 3076
  26.3 173.0 %copy-start.17 = (f32[768]{0:T(1024)}, f32[768]{0:T(1024)S(1)}, u32[]{:S(2)}) copy-start(f32[768]{0:T(1024)S(1)} %add_rsqrt_fusion.2) | copy-start | bytes 9220
  71.9 1.2 copy-start.3
  117.6 1.1 copy-start.4
  156.4 1.6 copy-start.12
  166.3 3.8 copy-start.5
  166.3 3.8 copy-start.10
  166.3 3.8 copy-start.11
  172.7 1.1 copy-start
  222.7 2.5 copy-start.8
  226.9 1.4 copy-start.7
  257.4 3.7 copy-start.9
  274.7 0.6 copy-start.19
  275.3 24.6 %copy-start.18 = (f32[768]{0:T(1024)S(1)}, f32[768]{0:T(1024)}, u32[]{:S(2)}) copy-start(f32[768]{0:T(1024)} %copy-done.17) | copy-start | bytes 9220
  275.8 24.1 %copy-start.1 = (bf16[768,2048]{1,0:T(8,128)(2,1)S(1)}, bf16[768,2048]{1,0:T(8,128)(2,1)}, u32[]{:S(2)}) copy-start(bf16[768,2048]{1,0:T(8,128)(2,1)} %all-gather.12.cloned.1.call-done) | copy-start | bytes 9437188
  308.0 2.1 copy-start.16
  308.0 2.2 copy-start.14
  308.0 2.2 copy-start.13
  308.0 123.7 %all-gather.26.cloned.1.call-start = ((), (), s32[]{:S(2)}) async-start(), calls=%async_computation.9 | async-start | bytes 7077888 | tf_op jit(solution)/shard_map/all_gather | solution.py:174
  308.8 221.9 %all-gather.28.cloned.1.call-start = ((), (), s32[]{:S(2)}) async-start(), calls=%async_computation.10 | async-start | bytes 7077888 | tf_op jit(solution)/shard_map/all_gather | solution.py:175
  309.3 320.4 %all-gather.30.cloned.1.call-start = ((), (), s32[]{:S(2)}) async-start(), calls=%async_computation.12 | async-start | bytes 7077888 | tf_op jit(solution)/shard_map/all_gather | solution.py:182
  310.1 355.7 %reduce-scatter.2.cloned.1.call-start = ((), (), s32[]{:S(2)}) async-start(), calls=%async_computation.11 | async-start | bytes 4718592 | tf_op jit(solution)/shard_map/reduce_scatter | solution.py:184
  440.6 90.0 %copy-start.2 = (bf16[768,2048]{1,0:T(8,128)(2,1)S(1)}, bf16[768,2048]{1,0:T(8,128)(2,1)}, u32[]{:S(2)}) copy-start(bf16[768,2048]{1,0:T(8,128)(2,1)} %get-tuple-element.166) | copy-start | bytes 9437188
  638.4 11.6 %copy-start.6 = (bf16[1536,8,256]{0,2,1:T(8,128)(2,1)S(1)}, bf16[1536,8,256]{0,2,1:T(8,128)(2,1)}, u32[]{:S(2)}) copy-start(bf16[1536,8,256]{0,2,1:T(8,128)(2,1)} %copy.99) | copy-start | bytes 18874372
Sparse Core Ops, SparseCore 0:
  8.9 14.8 all-gather.11
  25.9 41.4 all-gather.17
  69.5 38.9 all-gather.19
  110.5 38.9 all-gather.15
  151.5 47.7 all-gather.13
  201.3 47.6 all-gather.21
  251.0 48.8 all-gather.23
  308.1 21.4 all-reduce.3
  331.8 99.8 all-gather.25
  433.8 96.8 all-gather.27
  532.9 96.8 all-gather.29
  656.6 9.1 reduce-scatter.1
